TPU v7x, 32 devices: a whole 2x2x4 slice. The times are simulated.
32 devices in a mesh: sp: 4 (over z), fs: 4 (over y, x), tp: 2 (over core).
Axes of the slice: x: 2, y: 2, z: 4, core: 2. Of those that a mesh axis runs over, the one named last changes fastest.
Arguments:
- tokens: bfloat16 [4, 2048, 2048], P('fs', ('sp', 'tp')), may hold values from -6 to 6
- norm_gain: float32 [2048], replicated, may hold values from 0.1 to 1.9
- query_weight: bfloat16 [2048, 1024], P('sp', 'tp'), may hold values from -20 to 20
- key_matrix: bfloat16 [2048, 256], P('sp', 'tp'), may hold values from -0.125 to 0.125
- value_matrix: bfloat16 [2048, 256], P('sp', 'tp'), may hold values from -0.125 to 0.125
- pool_in_weight: bfloat16 [2048, 1024], P('sp', 'tp'), may hold values from -0.125 to 0.125
- head_sink_logit: float32 [16], replicated, may hold values from 2 to 6
- pool_mix: bfloat16 [4, 256, 256], replicated, may hold values from -0.375 to 0.375
- pool_gain: float32 [1024], replicated, may hold values from 0.1 to 1.9
- attn_out_weight: bfloat16 [1024, 2048], P('tp', 'sp'), may hold values from -1 to 1
- pool_out_weight: bfloat16 [1024, 2048], P('tp', 'sp'), may hold values from -0.125 to 0.125
Outputs:
- mixed: bfloat16 [4, 2048, 2048], P('fs', ('sp', 'tp'))
- row_log_weight_sum: float32 [4, 16, 2048], P('fs', 'tp', 'sp')
All inputs are finite; a program needn't handle non-finite values.
Results may differ from a plain program's by a relative error of at most 0.0095.
The roundings to bfloat16 on the way count: a program that leaves them out, or rounds other values in their place, can miss the bound.
Values may be sent and summed in bfloat16 or wider, within the bound.
No kernel may reach another device: no remote copies, remote signals or barrier semaphores. Data moves between devices by JAX's collectives and lax.ppermute only.
A program may use at most 64 MiB of HBM per device.

v0:
```python
import jax
import jax.numpy as jnp
from jax import lax
from jax.sharding import PartitionSpec as P

HEAD_SIZE = 64
WINDOW = 128
POOL_CH = 256
EPSILON = 1e-06
POOL_SPANS = (2, 4, 8, 16)


def passed_along(shard, axis, by):
    size = lax.axis_size(axis)
    pairs = [(i, i + by) for i in range(size) if 0 <= i + by < size]
    return lax.ppermute(shard, axis, pairs)


def windowed_attend(
    query_rows, key_rows, value_rows, key_tail, value_tail, sinks, kv_heads, group, first_pos
):
    rows = query_rows.shape[0]
    blocks = rows // WINDOW
    width = key_rows.shape[1]
    ext_keys = jnp.concatenate([key_tail, key_rows], 0)
    ext_values = jnp.concatenate([value_tail, value_rows], 0)

    def banded(table):
        return jnp.concatenate(
            [
                table[:rows].reshape(blocks, WINDOW, width),
                table[WINDOW:].reshape(blocks, WINDOW, width),
            ],
            axis=1,
        )

    band_keys = banded(ext_keys).reshape(blocks, 2 * WINDOW, kv_heads, HEAD_SIZE)
    band_values = banded(ext_values).reshape(blocks, 2 * WINDOW, kv_heads, HEAD_SIZE)
    query_blocks = query_rows.reshape(blocks, WINDOW, kv_heads, group, HEAD_SIZE)
    scores = jnp.einsum(
        "bqkgd,bskd->bkgqs", query_blocks, band_keys, preferred_element_type=jnp.float32
    ) * HEAD_SIZE ** (-0.5)
    query_pos = first_pos + jnp.arange(rows).reshape(blocks, WINDOW, 1)
    key_pos = (
        first_pos
        - WINDOW
        + jnp.arange(blocks).reshape(blocks, 1, 1) * WINDOW
        + jnp.arange(2 * WINDOW).reshape(1, 1, 2 * WINDOW)
    )
    offset = query_pos - key_pos
    allowed = (offset >= 0) & (offset < WINDOW) & (key_pos >= 0)
    scores = jnp.where(allowed[:, None, None], scores, -jnp.inf)
    sink_grid = sinks.reshape(1, kv_heads, group, 1, 1)
    top = jnp.maximum(jnp.max(scores, axis=-1, keepdims=True), sink_grid)
    weights = jnp.exp(scores - top)
    total = jnp.sum(weights, axis=-1, keepdims=True) + jnp.exp(sink_grid - top)
    probs = (weights / total).astype(jnp.bfloat16)
    mixed = jnp.einsum(
        "bkgqs,bskd->bqkgd", probs, band_values, preferred_element_type=jnp.float32
    ).astype(jnp.bfloat16)
    row_log_weight_sum = (top + jnp.log(total))[..., 0]
    return (
        mixed.reshape(rows, kv_heads * group * HEAD_SIZE),
        row_log_weight_sum.transpose(1, 2, 0, 3).reshape(kv_heads * group, rows),
    )


def pool_branch(pool_rows, pool_tail, mixing, scales, group_start, first_pos):
    rows = pool_rows.shape[0]
    columns = pool_rows.shape[1]
    pool_reach = max(POOL_SPANS)
    extended = jnp.concatenate([pool_tail, pool_rows], 0).astype(jnp.float32)
    group_index = group_start + jnp.arange(columns) // POOL_CH
    span_table = jnp.array(POOL_SPANS, jnp.int32)
    matches = group_index[:, None] == jnp.arange(len(POOL_SPANS))[None, :]
    span_of_col = jnp.sum(jnp.where(matches, span_table[None, :], 0), axis=1)
    trailing = jnp.zeros((rows, columns), jnp.float32)
    for lag in range(pool_reach):
        trailing = trailing + jnp.where(
            lag < span_of_col[None, :], extended[pool_reach - lag : pool_reach - lag + rows], 0.0
        )
    position = first_pos + jnp.arange(rows)
    count = jnp.minimum(position[:, None] + 1, span_of_col[None, :]).astype(jnp.float32)
    centred = (trailing / count - extended[pool_reach:]).astype(jnp.bfloat16)
    grouped = centred.reshape(rows, columns // POOL_CH, POOL_CH)
    product = jnp.einsum(
        "rgc,gcd->rgd", grouped, mixing, preferred_element_type=jnp.float32
    ).reshape(rows, columns)
    return (product * scales).astype(jnp.bfloat16)


def local(
    tokens,
    norm_gain,
    query_weight,
    key_matrix,
    value_matrix,
    pool_in_weight,
    head_sink_logit,
    pool_mix,
    pool_gain,
    attn_out_weight,
    pool_out_weight,
):
    tp_index = lax.axis_index("tp")
    sp_index = lax.axis_index("sp")
    q_cols = query_weight.shape[1]
    kv_cols = key_matrix.shape[1]
    pool_cols = pool_in_weight.shape[1]
    q_heads = q_cols // HEAD_SIZE
    kv_heads = kv_cols // HEAD_SIZE
    groups_dev = pool_cols // POOL_CH
    full_query, full_key, full_value, full_pool = (
        lax.all_gather(query_weight, "sp", axis=0, tiled=True),
        lax.all_gather(key_matrix, "sp", axis=0, tiled=True),
        lax.all_gather(value_matrix, "sp", axis=0, tiled=True),
        lax.all_gather(pool_in_weight, "sp", axis=0, tiled=True),
    )
    values_f = lax.all_gather(tokens[0], "tp", axis=0, tiled=True).astype(jnp.float32)
    scale = lax.rsqrt(jnp.mean(values_f * values_f, axis=-1, keepdims=True) + EPSILON)
    normed = (values_f * scale * norm_gain).astype(jnp.bfloat16)
    outputs = [
        jnp.dot(normed, weight, preferred_element_type=jnp.float32).astype(jnp.bfloat16)
        for weight in (full_query, full_key, full_value, full_pool)
    ]
    projected = jnp.concatenate(outputs, axis=1)
    rows = projected.shape[0]
    first_pos = sp_index * rows
    query_rows = projected[:, :q_cols]
    key_rows = projected[:, q_cols : q_cols + kv_cols]
    value_rows = projected[:, q_cols + kv_cols : q_cols + 2 * kv_cols]
    pool_rows = projected[:, q_cols + 2 * kv_cols :]
    pool_reach = max(POOL_SPANS)
    sinks = lax.dynamic_slice_in_dim(head_sink_logit, tp_index * q_heads, q_heads, 0)
    mixing = lax.dynamic_slice_in_dim(pool_mix, tp_index * groups_dev, groups_dev, 0)
    scales = lax.dynamic_slice_in_dim(pool_gain, tp_index * pool_cols, pool_cols, 0)
    key_tail, value_tail, pool_tail = passed_along(
        (key_rows[rows - WINDOW :], value_rows[rows - WINDOW :], pool_rows[rows - pool_reach :]),
        "sp",
        1,
    )
    attn_part, log_part = windowed_attend(
        query_rows,
        key_rows,
        value_rows,
        key_tail,
        value_tail,
        sinks,
        kv_heads,
        q_heads // kv_heads,
        first_pos,
    )
    pool_part = pool_branch(pool_rows, pool_tail, mixing, scales, tp_index * groups_dev, first_pos)
    half_attn, half_pool = (
        lax.all_gather(attn_out_weight, "sp", axis=1, tiled=True),
        lax.all_gather(pool_out_weight, "sp", axis=1, tiled=True),
    )
    result = lax.psum_scatter(
        jnp.dot(attn_part, half_attn, preferred_element_type=jnp.float32)
        + jnp.dot(pool_part, half_pool, preferred_element_type=jnp.float32),
        "tp",
        scatter_dimension=0,
        tiled=True,
    ).astype(jnp.bfloat16)
    return (result[None], log_part[None])


def solution(mesh):
    in_specs = (
        P("fs", ("sp", "tp"), None),
        P(),
        P("sp", "tp"),
        P("sp", "tp"),
        P("sp", "tp"),
        P("sp", "tp"),
        P(),
        P(),
        P(),
        P("tp", "sp"),
        P("tp", "sp"),
    )
    out_specs = (P("fs", ("sp", "tp"), None), P("fs", "tp", "sp"))
    return jax.shard_map(local, mesh=mesh, in_specs=in_specs, out_specs=out_specs, check_vma=False)
```

profile of v0, /device:TPU:0, one launch (start us, length us, event | category | flops | bytes accessed | tf_op | source)
XLA Modules:
  0.0 243.1 jit_solution(15689682092924149541)
XLA Ops:
  10.8 17.6 %all_gather.23 = bf16[2048,128]{1,0:T(8,128)(2,1)S(1)} all-gather(bf16[512,128]{1,0:T(8,128)(2,1)} %param.15), channel_id=1, replica_groups=mesh['sp'=4,'fs'=4,'tp'=2] {'sp'}, dimensions={0}, use_global_device_ids=true | all-gather | bytes 655360 | tf_op jit(solution)/shard_map/all_gather | solution.py:115
  29.2 23.4 %all_gather.22 = bf16[2048,128]{1,0:T(8,128)(2,1)} all-gather(bf16[512,128]{1,0:T(8,128)(2,1)} %param.16), channel_id=1, replica_groups=mesh['sp'=4,'fs'=4,'tp'=2] {'sp'}, dimensions={0}, use_global_device_ids=true | all-gather | bytes 655360 | tf_op jit(solution)/shard_map/all_gather | solution.py:116
  53.9 2.2 fusion
  56.1 2.4 convolution_convert_fusion.2
  59.1 3.5 %collective-permute-start.1 = (bf16[128,128]{1,0:T(8,128)(2,1)}, bf16[128,128]{1,0:T(8,128)(2,1)}, u32[]{:S(2)}, u32[]{:S(2)}) collective-permute-start(bf16[128,128]{1,0:T(8,128)(2,1)} %slice.86), channel_id=1, source_target_pairs={{0,8},{8,16},{16,24},{1,9},{9,17},{17,25},{2,10},{10,18},{18,26},{... | collective-permute-start | bytes 98312 | tf_op jit(solution)/shard_map/ppermute | solution.py:16
  62.6 1.5 convolution_convert_fusion.3
  65.0 0.8 copy.45
  65.8 2.0 collective-permute-start
  71.3 5.5 %all-gather.7.cloned.1.call-done = bf16[2048,512]{1,0:T(8,128)(2,1)} async-done(((bf16[512,512]{1,0:T(8,128)(2,1)}), bf16[2048,512]{1,0:T(8,128)(2,1)}) %all-gather.7.cloned.1.call-update) | async-done | bytes 2097168 | tf_op jit(solution)/shard_map/all_gather | solution.py:114
  76.8 2.9 %convolution_convert_fusion.1 = bf16[512,512]{1,0:T(8,128)(2,1)S(1)} fusion(bf16[2048,512]{1,0:T(8,128)(2,1)} %all-gather.7.cloned.1.call-done, bf16[1,512,2048]{2,1,0:T(8,128)(2,1)S(1)} %copy-done.1, f32[2048]{0:T(1024)} %param.13, f32[512]{0:T(512)} %copy-done.23), kind=kOutput, calls=%fused_computation.13 | convolution fusion | flops 1078198272 | bytes 4728832 | tf_op jit(solution)/shard_map/dot_general | solution.py:123
  79.7 1.5 reshape.236
  81.3 2.3 fusion.4
  83.6 1.0 fusion.3
  84.7 1.2 fusion.7
  86.3 38.3 %all-gather.11.cloned.1.call-done = bf16[2048,512]{1,0:T(8,128)(2,1)} async-done(((bf16[512,512]{1,0:T(8,128)(2,1)}), bf16[2048,512]{1,0:T(8,128)(2,1)}) %all-gather.11.cloned.1.call-update) | async-done | bytes 2097168 | tf_op jit(solution)/shard_map/all_gather | solution.py:117
  124.6 2.9 %convolution_convert_fusion = bf16[512,512]{1,0:T(8,128)(2,1)S(1)} fusion(bf16[2048,512]{1,0:T(8,128)(2,1)} %all-gather.11.cloned.1.call-done, bf16[1,512,2048]{2,1,0:T(8,128)(2,1)S(1)} %copy-done.1, f32[2048]{0:T(1024)S(1)} %copy-done.28, f32[512]{0:T(512)S(1)} %copy-done.24), kind=kOutput, calls=%fused_computation.12 | convolution fusion | flops 1078198272 | bytes 4728832 | tf_op jit(solution)/shard_map/dot_general | solution.py:123
  128.3 2.4 collective-permute-start.2
  130.7 39.8 %all-gather.9.cloned.1.call-done = bf16[512,2048]{1,0:T(8,128)(2,1)} async-done(((bf16[512,512]{1,0:T(8,128)(2,1)}), bf16[512,2048]{1,0:T(8,128)(2,1)}) %all-gather.9.cloned.1.call-update) | async-done | bytes 2097168 | tf_op jit(solution)/shard_map/all_gather | solution.py:155
  170.6 4.9 %fusion.29 = f32[512,2048]{1,0:T(8,128)} fusion(bf16[512,2048]{1,0:T(8,128)(2,1)} %all-gather.9.cloned.1.call-done, bf16[64,8,4,128]{3,2,1,0:T(4,128)(2,1)S(1)} %bitcast.76), kind=kOutput, calls=%fused_computation.59 | convolution fusion | flops 1073741824 | bytes 6815744 | tf_op jit(solution)/shard_map/dot_general | solution.py:159
  175.8 3.0 %fusion.28 = bf16[512,512]{1,0:T(8,128)(2,1)S(1)} fusion(f32[528,512]{1,0:T(8,128)S(1)} %maximum_convert_fusion, s32[512]{0:T(512)S(1)} %select_reduce_fusion, s32[512]{0:T(512)S(1)} %add_add_fusion, pred[512]{0:T(512)(128)(4,1)S(1)} %copy-done.8, pred[512]{0:T(512)(128)(4,1)S(1)} %copy-done.9, pred[512]{0:T(512)(128)(4,1)S(1)} %copy-done.10, ...), kind=kLoop, calls=%fused_computation.55 | loop fusion | flops 9437184 | bytes 17313792 | tf_op jit(solution)/shard_map/convert_element_type | solution.py:84
  179.3 37.1 %all-gather.13.cloned.1.call-done = bf16[512,2048]{1,0:T(8,128)(2,1)} async-done(((bf16[512,512]{1,0:T(8,128)(2,1)}), bf16[512,2048]{1,0:T(8,128)(2,1)}) %all-gather.13.cloned.1.call-update) | async-done | bytes 2097168 | tf_op jit(solution)/shard_map/all_gather | solution.py:156
  216.4 6.1 %convolution_add_fusion = f32[512,2048]{1,0:T(8,128)} fusion(f32[512,2048]{1,0:T(8,128)} %fusion.29, bf16[512,512]{0,1:T(8,128)(2,1)S(1)} %fusion.25, bf16[512,2048]{1,0:T(8,128)(2,1)} %all-gather.13.cloned.1.call-done), kind=kOutput, calls=%fused_computation.9 | convolution fusion | flops 1074790400 | bytes 11010048 | tf_op jit(solution)/shard_map/dot_general | solution.py:160
  223.2 10.3 %reduce-scatter.2.cloned.1.call-done = f32[256,2048]{1,0:T(8,128)} async-done(((f32[512,2048]{1,0:T(8,128)}), f32[256,2048]{1,0:T(8,128)}) %reduce-scatter.2.cloned.1.call-update) | async-done | bytes 2097168 | tf_op jit(solution)/shard_map/reduce_scatter | solution.py:158
  233.5 2.7 %convert_bitcast_fusion = bf16[1,256,2048]{2,1,0:T(8,128)(2,1)} fusion(f32[256,2048]{1,0:T(8,128)} %reduce-scatter.2.cloned.1.call-done), kind=kLoop, calls=%fused_computation.54 | loop fusion | flops 524288 | bytes 3145728 | tf_op jit(solution)/shard_map/broadcast_in_dim | solution.py:165
  (106 shorter events, 13.3 us)
Async XLA Ops:
  7.2 171.7 %copy-start = (bf16[4,256,256]{2,1,0:T(8,128)(2,1)S(1)}, bf16[4,256,256]{2,1,0:T(8,128)(2,1)}, u32[]{:S(2)}) copy-start(bf16[4,256,256]{2,1,0:T(8,128)(2,1)} %param.19) | copy-start | bytes 1572868
  7.2 45.5 %copy-start.26 = (s32[4]{0:T(128)S(1)}, s32[4]{0:T(128)}, u32[]{:S(2)}) copy-start(s32[4]{0:T(128)} %constant.89.clone) | copy-start | bytes 52
  7.2 46.2 %copy-start.25 = (f32[1024]{0:T(1024)S(1)}, f32[1024]{0:T(1024)}, u32[]{:S(2)}) copy-start(f32[1024]{0:T(1024)} %param.20) | copy-start | bytes 12292
  7.2 48.9 %copy-start.27 = (f32[2048]{0:T(1024)S(1)}, f32[2048]{0:T(1024)}, u32[]{:S(2)}) copy-start(f32[2048]{0:T(1024)} %param.13) | copy-start | bytes 24580
  7.2 46.6 %all-gather.15.cloned.1.call-start = ((), (), s32[]{:S(2)}) async-start(), calls=%async_computation.6 | async-start | bytes 3145728 | tf_op jit(solution)/shard_map/all_gather | solution.py:119
  7.9 68.9 %all-gather.7.cloned.1.call-start = ((), (), s32[]{:S(2)}) async-start(), calls=%async_computation.1 | async-start | bytes 2621440 | tf_op jit(solution)/shard_map/all_gather | solution.py:114
  8.7 115.9 %all-gather.11.cloned.1.call-start = ((), (), s32[]{:S(2)}) async-start(), calls=%async_computation.3 | async-start | bytes 2621440 | tf_op jit(solution)/shard_map/all_gather | solution.py:117
  9.4 161.1 %all-gather.9.cloned.1.call-start = ((), (), s32[]{:S(2)}) async-start(), calls=%async_computation.2 | async-start | bytes 2621440 | tf_op jit(solution)/shard_map/all_gather | solution.py:155
  10.0 206.4 %all-gather.13.cloned.1.call-start = ((), (), s32[]{:S(2)}) async-start(), calls=%async_computation.4 | async-start | bytes 2621440 | tf_op jit(solution)/shard_map/all_gather | solution.py:156
  10.6 222.9 %reduce-scatter.2.cloned.1.call-start = ((), (), s32[]{:S(2)}) async-start(), calls=%async_computation.5 | async-start | bytes 6291456 | tf_op jit(solution)/shard_map/reduce_scatter | solution.py:158
  53.8 8.8 %copy-start.1 = (bf16[1,512,2048]{2,1,0:T(8,128)(2,1)S(1)}, bf16[1,512,2048]{2,1,0:T(8,128)(2,1)}, u32[]{:S(2)}) copy-start(bf16[1,512,2048]{2,1,0:T(8,128)(2,1)} %all-gather.15.cloned.1.call-done) | copy-start | bytes 6291460
  53.8 8.8 %copy-start.4 = (bf16[2048,128]{1,0:T(8,128)(2,1)S(1)}, bf16[2048,128]{1,0:T(8,128)(2,1)}, u32[]{:S(2)}) copy-start(bf16[2048,128]{1,0:T(8,128)(2,1)} %all_gather.22) | copy-start | bytes 1572868
  56.1 6.5 %copy-start.23 = (f32[512]{0:T(512)}, f32[512]{0:T(512)S(1)}, u32[]{:S(2)}) copy-start(f32[512]{0:T(512)S(1)} %add_rsqrt_fusion) | copy-start | bytes 6148
  59.1 9.4 %collective-permute-start.1 = (bf16[128,128]{1,0:T(8,128)(2,1)}, bf16[128,128]{1,0:T(8,128)(2,1)}, u32[]{:S(2)}, u32[]{:S(2)}) collective-permute-start(bf16[128,128]{1,0:T(8,128)(2,1)} %slice.86), channel_id=1, source_target_pairs={{0,8},{8,16},{16,24},{1,9},{9,17},{17,25},{2,10},{10,18},{18,26},{... | collective-permute-start | bytes 98312 | tf_op jit(solution)/shard_map/ppermute | solution.py:16
  65.8 4.6 %collective-permute-start = (bf16[128,128]{1,0:T(8,128)(2,1)}, bf16[128,128]{1,0:T(8,128)(2,1)S(1)}, u32[]{:S(2)}, u32[]{:S(2)}) collective-permute-start(bf16[128,128]{1,0:T(8,128)(2,1)} %slice.85), channel_id=1, source_target_pairs={{0,8},{8,16},{16,24},{1,9},{9,17},{17,25},{2,10},{10,18},{18,26},{... | collective-permute-start | bytes 98312 | tf_op jit(solution)/shard_map/ppermute | solution.py:16
  84.7 39.9 %copy-start.24 = (f32[512]{0:T(512)S(1)}, f32[512]{0:T(512)}, u32[]{:S(2)}) copy-start(f32[512]{0:T(512)} %copy-done.23) | copy-start | bytes 6148
  84.7 39.9 %copy-start.28 = (f32[2048]{0:T(1024)S(1)}, f32[2048]{0:T(1024)}, u32[]{:S(2)}) copy-start(f32[2048]{0:T(1024)} %param.13) | copy-start | bytes 24580
  128.3 47.2 %copy-start.3 = (bf16[512,512]{1,0:T(8,128)(2,1)S(1)}, bf16[512,512]{1,0:T(8,128)(2,1)}, u32[]{:S(2)}) copy-start(bf16[512,512]{1,0:T(8,128)(2,1)} %copy-done.2) | copy-start | bytes 1572868
  128.3 47.2 %collective-permute-start.2 = (bf16[16,512]{1,0:T(8,128)(2,1)S(1)}, bf16[16,512]{1,0:T(8,128)(2,1)S(1)}, u32[]{:S(2)}, u32[]{:S(2)}) collective-permute-start(bf16[16,512]{1,0:T(8,128)(2,1)S(1)} %slice.87), channel_id=1, source_target_pairs={{0,8},{8,16},{16,24},{1,9},{9,17},{17,25},{2,10},{10,18},{18,26},{... | collective-permute-start | bytes 49160 | tf_op jit(solution)/shard_map/ppermute | solution.py:16
  170.5 5.2 %copy-start.12 = (pred[512]{0:T(512)(128)(4,1)S(1)}, pred[512]{0:T(512)(128)(4,1)}, u32[]{:S(2)}) copy-start(pred[512]{0:T(512)(128)(4,1)} %get-tuple-element.7) | copy-start | bytes 1540
  170.5 5.2 %copy-start.13 = (pred[512]{0:T(512)(128)(4,1)S(1)}, pred[512]{0:T(512)(128)(4,1)}, u32[]{:S(2)}) copy-start(pred[512]{0:T(512)(128)(4,1)} %get-tuple-element.8) | copy-start | bytes 1540
  170.6 5.2 %copy-start.14 = (pred[512]{0:T(512)(128)(4,1)S(1)}, pred[512]{0:T(512)(128)(4,1)}, u32[]{:S(2)}) copy-start(pred[512]{0:T(512)(128)(4,1)} %get-tuple-element.9) | copy-start | bytes 1540
  170.6 5.2 %copy-start.15 = (pred[512]{0:T(512)(128)(4,1)S(1)}, pred[512]{0:T(512)(128)(4,1)}, u32[]{:S(2)}) copy-start(pred[512]{0:T(512)(128)(4,1)} %get-tuple-element.10) | copy-start | bytes 1540
  170.6 5.2 %copy-start.16 = (pred[512]{0:T(512)(128)(4,1)S(1)}, pred[512]{0:T(512)(128)(4,1)}, u32[]{:S(2)}) copy-start(pred[512]{0:T(512)(128)(4,1)} %get-tuple-element.11) | copy-start | bytes 1540
  (14 other events, 64.3 us)
Sparse Core Ops, SparseCore 0:
  9.6 13.2 all-gather.14
  24.5 52.2 all-gather.6
  78.4 46.1 all-gather.10
  126.0 44.4 all-gather.8
  171.9 44.4 all-gather.12
  222.7 10.8 reduce-scatter.1
where the time goes:
time: 244 us; the launch traced here: 243 us
  waiting for transfers between devices  134 us (55%)
  blocking collectives  41 us (17%)
  matrix products  24.4 us (10%)
  between operations  14.6 us (6%)
  other arithmetic  12.1 us (5%)
  local copies, waits for them, and re-layouts  8.64 us (4%)
  starting transfers between devices  8.09 us (3%)
    all_gather x1, waiting for transfers between devices, local(): lax.all_gather(attn_out_weight, 'sp', axis=1, tiled=True)  39.8 us
    all_gather x1, waiting for transfers between devices, local(): lax.all_gather(pool_in_weight, 'sp', axis=0, tiled=True)  38.3 us
    all_gather x1, waiting for transfers between devices, local(): lax.all_gather(pool_out_weight, 'sp', axis=1, tiled=True)  37.1 us
    all_gather x1, blocking collectives, local(): lax.all_gather(value_matrix, 'sp', axis=0, tiled=True)  23.4 us
    all_gather x1, blocking collectives, local(): lax.all_gather(key_matrix, 'sp', axis=0, tiled=True)  17.6 us
    reduce_scatter x1, waiting for transfers between devices, local(): lax.psum_scatter(jnp.dot(attn_part, half_attn, preferred_element_type=jnp...  10.3 us
    dot_general x4, matrix products, local(): jnp.dot(normed, weight, preferred_element_type=jnp.float32)  9.63 us
    ppermute x3, starting transfers between devices, passed_along(): return lax.ppermute(shard, axis, pairs)  7.87 us
  transfers between devices with their start and end apart: 9, of which 6 were waited for; matrix products, arithmetic and copies ran while one was open for 15% of the time, Pallas kernels for 0%

commit v1 on v0

--- a/solution.py
+++ b/solution.py
@@ -153,7 +153,7 @@
     pool_part = pool_branch(pool_rows, pool_tail, mixing, scales, tp_index * groups_dev, first_pos)
     half_attn, half_pool = (
         lax.all_gather(attn_out_weight, "sp", axis=1, tiled=True),
-        lax.all_gather(pool_out_weight, "sp", axis=1, tiled=True),
+        jnp.concatenate(lax.all_gather(pool_out_weight, "sp"), axis=1),
     )
     result = lax.psum_scatter(
         jnp.dot(attn_part, half_attn, preferred_element_type=jnp.float32)

time: 244 us -> 247 us (1.012)
  waiting for transfers between devices: 134 us -> 138 us
  local copies, waits for them, and re-layouts: 8.64 us -> 12.1 us
  matrix products: 24.4 us -> 21.7 us
    all_gather x1, waiting for transfers between devices: 37.1 us -> 40.9 us  [local(): lax.all_gather(pool_out_weight, 'sp')]
    reshape x0 -> x1, local copies, waits for them, and re-layouts: none -> 2.79 us  [local(): jnp.concatenate(lax.all_gather(pool_out_weight, 'sp'), axis=1)]
    dot_general x1, matrix products: 6.08 us -> 3.33 us  [local(): jnp.dot(pool_part, half_pool, preferred_element_type=jnp.float32)]
  transfers between devices with their start and end apart: 9 -> 9, of which waited for: 6 -> 6; matrix products, arithmetic and copies ran while one was open for 15% -> 14% of each run, Pallas kernels for 0% -> 0%
where the time goes in v1:
time: 247 us
  waiting for transfers between devices  138 us (56%)
  blocking collectives  41 us (17%)
  matrix products  21.7 us (9%)
  between operations  14.7 us (6%)
  local copies, waits for them, and re-layouts  12.1 us (5%)
  other arithmetic  11.9 us (5%)
  starting transfers between devices  7.95 us (3%)
    all_gather x1, waiting for transfers between devices, local(): lax.all_gather(pool_out_weight, 'sp')  40.9 us
    all_gather x1, waiting for transfers between devices, local(): lax.all_gather(attn_out_weight, 'sp', axis=1, tiled=True)  40 us
    all_gather x1, waiting for transfers between devices, local(): lax.all_gather(pool_in_weight, 'sp', axis=0, tiled=True)  38.3 us
    all_gather x1, blocking collectives, local(): lax.all_gather(value_matrix, 'sp', axis=0, tiled=True)  23.4 us
    all_gather x1, blocking collectives, local(): lax.all_gather(key_matrix, 'sp', axis=0, tiled=True)  17.6 us
    reduce_scatter x1, waiting for transfers between devices, local(): lax.psum_scatter(jnp.dot(attn_part, half_attn, preferred_element_type=jnp...  10.3 us
    dot_general x4, matrix products, local(): jnp.dot(normed, weight, preferred_element_type=jnp.float32)  9.65 us
    ppermute x3, starting transfers between devices, passed_along(): return lax.ppermute(shard, axis, pairs)  7.72 us
  transfers between devices with their start and end apart: 9, of which 6 were waited for; matrix products, arithmetic and copies ran while one was open for 14% of the time, Pallas kernels for 0%

profile of v1, /device:TPU:0, one launch (start us, length us, event | category | flops | bytes accessed | tf_op | source)
XLA Modules:
  0.0 246.9 jit_solution(6794155017344855070)
XLA Ops:
  10.8 17.6 %all_gather.26 = bf16[2048,128]{1,0:T(8,128)(2,1)S(1)} all-gather(bf16[512,128]{1,0:T(8,128)(2,1)} %param.15), channel_id=1, replica_groups=mesh['sp'=4,'fs'=4,'tp'=2] {'sp'}, dimensions={0}, use_global_device_ids=true | all-gather | bytes 655360 | tf_op jit(solution)/shard_map/all_gather | solution.py:115
  29.2 23.4 %all_gather.25 = bf16[2048,128]{1,0:T(8,128)(2,1)} all-gather(bf16[512,128]{1,0:T(8,128)(2,1)} %param.16), channel_id=1, replica_groups=mesh['sp'=4,'fs'=4,'tp'=2] {'sp'}, dimensions={0}, use_global_device_ids=true | all-gather | bytes 655360 | tf_op jit(solution)/shard_map/all_gather | solution.py:116
  54.5 2.2 fusion
  56.7 2.4 convolution_convert_fusion.2
  59.7 3.5 %collective-permute-start.1 = (bf16[128,128]{1,0:T(8,128)(2,1)}, bf16[128,128]{1,0:T(8,128)(2,1)}, u32[]{:S(2)}, u32[]{:S(2)}) collective-permute-start(bf16[128,128]{1,0:T(8,128)(2,1)} %slice.86), channel_id=1, source_target_pairs={{0,8},{8,16},{16,24},{1,9},{9,17},{17,25},{2,10},{10,18},{18,26},{... | collective-permute-start | bytes 98312 | tf_op jit(solution)/shard_map/ppermute | solution.py:16
  63.2 1.5 convolution_convert_fusion.3
  66.4 2.0 collective-permute-start
  71.9 4.9 %all-gather.8.cloned.1.call-done = bf16[2048,512]{1,0:T(8,128)(2,1)} async-done(((bf16[512,512]{1,0:T(8,128)(2,1)}), bf16[2048,512]{1,0:T(8,128)(2,1)}) %all-gather.8.cloned.1.call-update) | async-done | bytes 2097168 | tf_op jit(solution)/shard_map/all_gather | solution.py:114
  76.8 2.9 %convolution_convert_fusion.1 = bf16[512,512]{1,0:T(8,128)(2,1)S(1)} fusion(bf16[2048,512]{1,0:T(8,128)(2,1)} %all-gather.8.cloned.1.call-done, bf16[1,512,2048]{2,1,0:T(8,128)(2,1)S(1)} %copy-done.2, f32[2048]{0:T(1024)} %param.13, f32[512]{0:T(512)} %copy-done.24), kind=kOutput, calls=%fused_computation.14 | convolution fusion | flops 1078198272 | bytes 4728832 | tf_op jit(solution)/shard_map/dot_general | solution.py:123
  79.7 1.5 reshape.248
  81.3 2.3 fusion.4
  83.6 1.0 fusion.3
  84.7 1.2 fusion.8
  86.3 38.3 %all-gather.12.cloned.1.call-done = bf16[2048,512]{1,0:T(8,128)(2,1)} async-done(((bf16[512,512]{1,0:T(8,128)(2,1)}), bf16[2048,512]{1,0:T(8,128)(2,1)}) %all-gather.12.cloned.1.call-update) | async-done | bytes 2097168 | tf_op jit(solution)/shard_map/all_gather | solution.py:117
  124.6 2.9 %convolution_convert_fusion = bf16[512,512]{1,0:T(8,128)(2,1)S(1)} fusion(bf16[2048,512]{1,0:T(8,128)(2,1)} %all-gather.12.cloned.1.call-done, bf16[1,512,2048]{2,1,0:T(8,128)(2,1)S(1)} %copy-done.2, f32[2048]{0:T(1024)S(1)} %copy-done.29, f32[512]{0:T(512)S(1)} %copy-done.25), kind=kOutput, calls=%fused_computation.13 | convolution fusion | flops 1078198272 | bytes 4728832 | tf_op jit(solution)/shard_map/dot_general | solution.py:123
  128.3 2.2 collective-permute-start.2
  130.6 40.0 %all-gather.10.cloned.1.call-done = bf16[512,2048]{1,0:T(8,128)(2,1)} async-done(((bf16[512,512]{1,0:T(8,128)(2,1)}), bf16[512,2048]{1,0:T(8,128)(2,1)}) %all-gather.10.cloned.1.call-update) | async-done | bytes 2097168 | tf_op jit(solution)/shard_map/all_gather | solution.py:155
  170.5 4.8 %fusion.29 = f32[512,2048]{1,0:T(8,128)} fusion(bf16[512,2048]{1,0:T(8,128)(2,1)} %all-gather.10.cloned.1.call-done, bf16[64,8,4,128]{3,2,1,0:T(4,128)(2,1)S(1)} %bitcast.78), kind=kOutput, calls=%fused_computation.59 | convolution fusion | flops 1073741824 | bytes 6815744 | tf_op jit(solution)/shard_map/dot_general | solution.py:159
  175.5 40.9 %all-gather.16.cloned.1.call-done = bf16[2048,512]{1,0:T(8,128)(2,1)} async-done(((bf16[512,512]{1,0:T(8,128)(2,1)}), bf16[2048,512]{1,0:T(8,128)(2,1)}) %all-gather.16.cloned.1.call-update) | async-done | bytes 2097168 | tf_op jit(solution)/shard_map/all_gather | solution.py:156
  216.4 2.8 %copy.68 = bf16[512,4,512]{0,2,1:T(8,128)(2,1)S(1)} copy(bf16[512,4,512]{2,0,1:T(8,128)(2,1)} %bitcast.77) | data formatting | bytes 4194304 | tf_op jit(solution)/shard_map/reshape | solution.py:156
  219.6 3.0 %fusion.28 = bf16[512,512]{1,0:T(8,128)(2,1)S(1)} fusion(f32[528,512]{1,0:T(8,128)S(1)} %maximum_convert_fusion, s32[512]{0:T(512)S(1)} %select_reduce_fusion, s32[512]{0:T(512)S(1)} %add_add_fusion, pred[512]{0:T(512)(128)(4,1)S(1)} %copy-done.8, pred[512]{0:T(512)(128)(4,1)S(1)} %copy-done.9, pred[512]{0:T(512)(128)(4,1)S(1)} %copy-done.10, ...), kind=kLoop, calls=%fused_computation.55 | loop fusion | flops 9437184 | bytes 17313792 | tf_op jit(solution)/shard_map/convert_element_type | solution.py:84
  223.0 3.3 %convolution_add_fusion = f32[512,2048]{1,0:T(8,128)} fusion(f32[512,2048]{1,0:T(8,128)S(1)} %copy-done.1, bf16[512,512]{0,1:T(8,128)(2,1)S(1)} %bitcast.80, bf16[512,2048]{0,1:T(8,128)(2,1)S(1)} %bitcast.76), kind=kOutput, calls=%fused_computation.9 | convolution fusion | flops 1074790400 | bytes 11010048 | tf_op jit(solution)/shard_map/dot_general | solution.py:160
  227.0 10.3 %reduce-scatter.2.cloned.1.call-done = f32[256,2048]{1,0:T(8,128)} async-done(((f32[512,2048]{1,0:T(8,128)}), f32[256,2048]{1,0:T(8,128)}) %reduce-scatter.2.cloned.1.call-update) | async-done | bytes 2097168 | tf_op jit(solution)/shard_map/reduce_scatter | solution.py:158
  237.3 2.7 %convert_bitcast_fusion = bf16[1,256,2048]{2,1,0:T(8,128)(2,1)} fusion(f32[256,2048]{1,0:T(8,128)} %reduce-scatter.2.cloned.1.call-done), kind=kLoop, calls=%fused_computation.54 | loop fusion | flops 524288 | bytes 3145728 | tf_op jit(solution)/shard_map/broadcast_in_dim | solution.py:165
  (109 shorter events, 14.6 us)
Async XLA Ops:
  7.2 215.4 %copy-start = (bf16[4,256,256]{2,1,0:T(8,128)(2,1)S(1)}, bf16[4,256,256]{2,1,0:T(8,128)(2,1)}, u32[]{:S(2)}) copy-start(bf16[4,256,256]{2,1,0:T(8,128)(2,1)} %param.19) | copy-start | bytes 1572868
  7.2 45.5 %copy-start.27 = (s32[4]{0:T(128)S(1)}, s32[4]{0:T(128)}, u32[]{:S(2)}) copy-start(s32[4]{0:T(128)} %constant.89.clone) | copy-start | bytes 52
  7.2 46.2 %copy-start.26 = (f32[1024]{0:T(1024)S(1)}, f32[1024]{0:T(1024)}, u32[]{:S(2)}) copy-start(f32[1024]{0:T(1024)} %param.20) | copy-start | bytes 12292
  7.2 49.5 %copy-start.28 = (f32[2048]{0:T(1024)S(1)}, f32[2048]{0:T(1024)}, u32[]{:S(2)}) copy-start(f32[2048]{0:T(1024)} %param.13) | copy-start | bytes 24580
  7.2 47.2 %all-gather.14.cloned.1.call-start = ((), (), s32[]{:S(2)}) async-start(), calls=%async_computation.5 | async-start | bytes 3145728 | tf_op jit(solution)/shard_map/all_gather | solution.py:119
  7.9 68.9 %all-gather.8.cloned.1.call-start = ((), (), s32[]{:S(2)}) async-start(), calls=%async_computation.1 | async-start | bytes 2621440 | tf_op jit(solution)/shard_map/all_gather | solution.py:114
  8.7 115.9 %all-gather.12.cloned.1.call-start = ((), (), s32[]{:S(2)}) async-start(), calls=%async_computation.3 | async-start | bytes 2621440 | tf_op jit(solution)/shard_map/all_gather | solution.py:117
  9.4 161.1 %all-gather.10.cloned.1.call-start = ((), (), s32[]{:S(2)}) async-start(), calls=%async_computation.2 | async-start | bytes 2621440 | tf_op jit(solution)/shard_map/all_gather | solution.py:155
  10.0 206.4 %all-gather.16.cloned.1.call-start = ((), (), s32[]{:S(2)}) async-start(), calls=%async_computation.6 | async-start | bytes 2621440 | tf_op jit(solution)/shard_map/all_gather | solution.py:156
  10.6 226.7 %reduce-scatter.2.cloned.1.call-start = ((), (), s32[]{:S(2)}) async-start(), calls=%async_computation.4 | async-start | bytes 6291456 | tf_op jit(solution)/shard_map/reduce_scatter | solution.py:158
  59.7 9.5 %collective-permute-start.1 = (bf16[128,128]{1,0:T(8,128)(2,1)}, bf16[128,128]{1,0:T(8,128)(2,1)}, u32[]{:S(2)}, u32[]{:S(2)}) collective-permute-start(bf16[128,128]{1,0:T(8,128)(2,1)} %slice.86), channel_id=1, source_target_pairs={{0,8},{8,16},{16,24},{1,9},{9,17},{17,25},{2,10},{10,18},{18,26},{... | collective-permute-start | bytes 98312 | tf_op jit(solution)/shard_map/ppermute | solution.py:16
  66.4 4.6 %collective-permute-start = (bf16[128,128]{1,0:T(8,128)(2,1)}, bf16[128,128]{1,0:T(8,128)(2,1)S(1)}, u32[]{:S(2)}, u32[]{:S(2)}) collective-permute-start(bf16[128,128]{1,0:T(8,128)(2,1)} %slice.85), channel_id=1, source_target_pairs={{0,8},{8,16},{16,24},{1,9},{9,17},{17,25},{2,10},{10,18},{18,26},{... | collective-permute-start | bytes 98312 | tf_op jit(solution)/shard_map/ppermute | solution.py:16
  128.3 90.9 %collective-permute-start.2 = (bf16[16,512]{1,0:T(8,128)(2,1)S(1)}, bf16[16,512]{1,0:T(8,128)(2,1)S(1)}, u32[]{:S(2)}, u32[]{:S(2)}) collective-permute-start(bf16[16,512]{1,0:T(8,128)(2,1)S(1)} %slice.87), channel_id=1, source_target_pairs={{0,8},{8,16},{16,24},{1,9},{9,17},{17,25},{2,10},{10,18},{18,26},{... | collective-permute-start | bytes 49160 | tf_op jit(solution)/shard_map/ppermute | solution.py:16
  175.4 44.0 %copy-start.11 = (pred[512]{0:T(512)(128)(4,1)S(1)}, pred[512]{0:T(512)(128)(4,1)}, u32[]{:S(2)}) copy-start(pred[512]{0:T(512)(128)(4,1)} %get-tuple-element.6) | copy-start | bytes 1540
  175.4 44.0 %copy-start.12 = (pred[512]{0:T(512)(128)(4,1)S(1)}, pred[512]{0:T(512)(128)(4,1)}, u32[]{:S(2)}) copy-start(pred[512]{0:T(512)(128)(4,1)} %get-tuple-element.7) | copy-start | bytes 1540
  175.4 44.0 %copy-start.13 = (pred[512]{0:T(512)(128)(4,1)S(1)}, pred[512]{0:T(512)(128)(4,1)}, u32[]{:S(2)}) copy-start(pred[512]{0:T(512)(128)(4,1)} %get-tuple-element.8) | copy-start | bytes 1540
  175.4 44.0 %copy-start.14 = (pred[512]{0:T(512)(128)(4,1)S(1)}, pred[512]{0:T(512)(128)(4,1)}, u32[]{:S(2)}) copy-start(pred[512]{0:T(512)(128)(4,1)} %get-tuple-element.9) | copy-start | bytes 1540
  175.4 44.0 %copy-start.15 = (pred[512]{0:T(512)(128)(4,1)S(1)}, pred[512]{0:T(512)(128)(4,1)}, u32[]{:S(2)}) copy-start(pred[512]{0:T(512)(128)(4,1)} %get-tuple-element.10) | copy-start | bytes 1540
  175.4 44.0 %copy-start.16 = (pred[512]{0:T(512)(128)(4,1)S(1)}, pred[512]{0:T(512)(128)(4,1)}, u32[]{:S(2)}) copy-start(pred[512]{0:T(512)(128)(4,1)} %get-tuple-element.11) | copy-start | bytes 1540
  175.4 44.0 %copy-start.17 = (pred[512]{0:T(512)(128)(4,1)S(1)}, pred[512]{0:T(512)(128)(4,1)}, u32[]{:S(2)}) copy-start(pred[512]{0:T(512)(128)(4,1)} %get-tuple-element.12) | copy-start | bytes 1540
  175.4 44.0 %copy-start.18 = (pred[512]{0:T(512)(128)(4,1)S(1)}, pred[512]{0:T(512)(128)(4,1)}, u32[]{:S(2)}) copy-start(pred[512]{0:T(512)(128)(4,1)} %get-tuple-element.13) | copy-start | bytes 1540
  175.5 44.0 %copy-start.19 = (pred[512]{0:T(512)(128)(4,1)S(1)}, pred[512]{0:T(512)(128)(4,1)}, u32[]{:S(2)}) copy-start(pred[512]{0:T(512)(128)(4,1)} %get-tuple-element.14) | copy-start | bytes 1540
  175.5 44.0 %copy-start.20 = (pred[512]{0:T(512)(128)(4,1)S(1)}, pred[512]{0:T(512)(128)(4,1)}, u32[]{:S(2)}) copy-start(pred[512]{0:T(512)(128)(4,1)} %get-tuple-element.15) | copy-start | bytes 1540
  175.5 44.0 %copy-start.21 = (pred[512]{0:T(512)(128)(4,1)S(1)}, pred[512]{0:T(512)(128)(4,1)}, u32[]{:S(2)}) copy-start(pred[512]{0:T(512)(128)(4,1)} %get-tuple-element.16) | copy-start | bytes 1540
  (15 other events, 338.0 us)
Sparse Core Ops, SparseCore 0:
  9.6 13.2 all-gather.13
  24.5 52.2 all-gather.7
  78.4 46.1 all-gather.11
  126.0 44.4 all-gather.9
  171.9 44.4 all-gather.15
  226.5 10.8 reduce-scatter.1
